TPU v7x, 32 devices: a whole 2x2x4 slice. The times are simulated.
32 devices in a mesh: row: 8 (over z, x), col: 4 (over y, core).
Axes of the slice: x: 2, y: 2, z: 4, core: 2. Of those that a mesh axis runs over, the one named last changes fastest.
Arguments:
- tokens: bfloat16 [2048, 2048], P('row'), may hold values from -6 to 6
- norm_gain: float32 [2048], replicated, may hold values from 0.5 to 1.5
- first_gate: bfloat16 [2048, 1024], P(None, 'col'), may hold values from -0.125 to 0.125
- second_gate: bfloat16 [2048, 1024], P(None, 'col'), may hold values from -0.125 to 0.125
- value_weight: bfloat16 [2048, 1024], P(None, 'col'), may hold values from -0.125 to 0.125
- short_weight: bfloat16 [3, 3, 1024], P(None, None, 'col'), may hold values from -3.5 to 3.5
- short_bias: float32 [3, 1024], P(None, 'col'), may hold values from -2 to 2
- embed_weight: float32 [33, 64], replicated, may hold values from -1 to 1
- embed_bias: float32 [64], replicated, may hold values from -3 to 3
- inner_weight: float32 [64, 64], replicated, may hold values from -0.75 to 0.75
- inner_bias: float32 [64], replicated, may hold values from -3 to 3
- filter_freq: float32 [64], replicated, may hold values from 0.5 to 1.5
- filter_weight: float32 [2, 2, 64, 1024], P(None, None, None, ('col', 'row')), may hold values from -0.046875 to 0.046875
- filter_skip: float32 [2, 1024], P(None, ('col', 'row')), may hold values from -3 to 3
- output_gain: float32 [1024], P('col'), may hold values from 0.5 to 1.5
- output_weight: bfloat16 [1024, 2048], replicated, may hold values from -0.1875 to 0.1875
Outputs:
- mixed_output: bfloat16 [2048, 2048], P(('row', 'col'))
All inputs are finite; a program needn't handle non-finite values.
Results may differ from a plain program's by a relative error of at most 0.01.
Values may be sent and summed in bfloat16 or wider, within the bound.
A program may use at most 64 MiB of HBM per device.

v0:
```python
import functools
import math

import jax
import jax.numpy as jnp
import numpy as np
from jax import lax
from jax.experimental import pallas as pl
from jax.experimental.pallas import tpu as pltpu
from jax.sharding import PartitionSpec as P

CHANNELS = 1024
GROUPS = 8
FREQ_BANDS = 16


HIGHEST = lax.Precision.HIGHEST
NORM_EPS = 1e-06
DECAY_TARGET = 0.01
FAST_SPAN = 0.3
SLOW_SPAN = 1.5


def for_sending(value):
    return jax.tree.map(lambda a: a.astype(jnp.bfloat16) if a.dtype == jnp.float32 else a, value)


def position_features(length):
    position_ramp = jnp.linspace(0.0, 1.0, length, dtype=jnp.float32)[:, None]
    angles = 2.0 * math.pi * jnp.arange(length, dtype=jnp.float32)[:, None] / length
    band_freqs = jnp.linspace(0.0001, FREQ_BANDS - 1, FREQ_BANDS, dtype=jnp.float32)[None, :]
    features = jnp.concatenate(
        [position_ramp, jnp.cos(band_freqs * angles), -jnp.sin(band_freqs * angles)], axis=1
    )
    return (position_ramp, features)


def filter_hidden(length, embed_weight, embed_bias, inner_weight, inner_bias, filter_freq):
    position_ramp, features = position_features(length)
    hidden = jnp.sin(
        filter_freq * (jnp.dot(features, embed_weight, precision=HIGHEST) + embed_bias)
    )
    hidden = jnp.sin(filter_freq * (jnp.dot(hidden, inner_weight, precision=HIGHEST) + inner_bias))
    return (position_ramp, hidden)


def decay_rates():
    fastest = math.log(DECAY_TARGET) / FAST_SPAN
    slowest = math.log(DECAY_TARGET) / SLOW_SPAN
    return jnp.abs(jnp.linspace(slowest, fastest, CHANNELS, dtype=jnp.float32))


def short_filter(padded, weights, bias_row, length):
    result = bias_row.astype(jnp.float32)
    for tap_index in range(weights.shape[0]):
        result = result + padded[tap_index : tap_index + length].astype(jnp.float32) * weights[
            tap_index
        ].astype(jnp.float32)
    return result


def phase_table(rows, cols, period):
    phase_index = (
        lax.broadcasted_iota(jnp.int32, (rows, cols), 0)
        * lax.broadcasted_iota(jnp.int32, (rows, cols), 1)
        % period
    )
    phase_angle = phase_index.astype(jnp.float32) * (2.0 * math.pi / period)
    return (jnp.cos(phase_angle), jnp.sin(phase_angle))


def split_length(total_size):
    chosen = 2
    for candidate in range(2, math.isqrt(total_size) + 1, 2):
        if total_size % candidate == 0:
            chosen = candidate
    return chosen


def make_tables(total_size):
    major_size = split_length(total_size)
    minor_size = total_size // major_size
    inner_table = phase_table(major_size, major_size, major_size)
    twiddle = phase_table(major_size, minor_size, total_size)
    outer_table = phase_table(minor_size, minor_size, minor_size)
    return (major_size, minor_size, inner_table, twiddle, outer_table)


def finish_forward(part_real, part_imag, twiddle, outer_table):
    turn_cos = twiddle[0][:, :, None]
    turn_sin = twiddle[1][:, :, None]
    turned_real = part_real * turn_cos + part_imag * turn_sin
    turned_imag = part_imag * turn_cos - part_real * turn_sin
    outer_cos, outer_sin = outer_table
    spec_real = jnp.einsum("anc,nk->akc", turned_real, outer_cos, precision=HIGHEST) + jnp.einsum(
        "anc,nk->akc", turned_imag, outer_sin, precision=HIGHEST
    )
    spec_imag = jnp.einsum("anc,nk->akc", turned_imag, outer_cos, precision=HIGHEST) - jnp.einsum(
        "anc,nk->akc", turned_real, outer_sin, precision=HIGHEST
    )
    return (spec_real, spec_imag)


def forward_signal(signal, tables):
    major_size, minor_size, inner_table, twiddle, outer_table = tables
    channels = signal.shape[1]
    flattened = signal.reshape(major_size // 2, minor_size * channels)
    inner_cos = inner_table[0][:, : major_size // 2]
    inner_sin = inner_table[1][:, : major_size // 2]
    part_real = jnp.dot(inner_cos, flattened, precision=HIGHEST).reshape(
        major_size, minor_size, channels
    )
    part_imag = -jnp.dot(inner_sin, flattened, precision=HIGHEST).reshape(
        major_size, minor_size, channels
    )
    return finish_forward(part_real, part_imag, twiddle, outer_table)


def forward_taps(circular_taps, tables):
    major_size, minor_size, inner_table, twiddle, outer_table = tables
    channels = circular_taps.shape[1]
    flattened = circular_taps.reshape(major_size, minor_size * channels)
    part_real = jnp.dot(inner_table[0], flattened, precision=HIGHEST).reshape(
        major_size, minor_size, channels
    )
    part_imag = -jnp.dot(inner_table[1], flattened, precision=HIGHEST).reshape(
        major_size, minor_size, channels
    )
    return finish_forward(part_real, part_imag, twiddle, outer_table)


def inverse(spec_real, spec_imag, tables):
    major_size, minor_size, inner_table, twiddle, outer_table = tables
    channels = spec_real.shape[2]
    outer_cos, outer_sin = outer_table
    back_real = jnp.einsum("akc,kn->anc", spec_real, outer_cos, precision=HIGHEST) - jnp.einsum(
        "akc,kn->anc", spec_imag, outer_sin, precision=HIGHEST
    )
    back_imag = jnp.einsum("akc,kn->anc", spec_imag, outer_cos, precision=HIGHEST) + jnp.einsum(
        "akc,kn->anc", spec_real, outer_sin, precision=HIGHEST
    )
    turn_cos = twiddle[0][:, :, None]
    turn_sin = twiddle[1][:, :, None]
    turned_real = (back_real * turn_cos - back_imag * turn_sin).reshape(
        major_size, minor_size * channels
    )
    turned_imag = (back_imag * turn_cos + back_real * turn_sin).reshape(
        major_size, minor_size * channels
    )
    half_rows = major_size // 2
    values = jnp.dot(inner_table[0][:half_rows], turned_real, precision=HIGHEST) - jnp.dot(
        inner_table[1][:half_rows], turned_imag, precision=HIGHEST
    )
    return values.reshape(half_rows * minor_size, channels) / (major_size * minor_size)


def two_sided(signal, forward, backward, skip_gain, tables):
    circular_taps = jnp.concatenate([forward, jnp.zeros_like(forward[:1]), backward[:0:-1]], axis=0)
    signal_real, signal_imag = forward_signal(signal, tables)
    taps_real, taps_imag = forward_taps(circular_taps, tables)
    prod_real = signal_real * taps_real - signal_imag * taps_imag
    prod_imag = signal_real * taps_imag + signal_imag * taps_real
    return inverse(prod_real, prod_imag, tables) + signal * skip_gain


def channel_taps(hidden, position_ramp, filter_weight, deltas):
    window = jnp.exp(-position_ramp * deltas[None, :])
    pairs = []
    for order_index in range(filter_weight.shape[0]):
        forward = jnp.dot(hidden, filter_weight[order_index, 0], precision=HIGHEST) * window
        backward = jnp.dot(hidden, filter_weight[order_index, 1], precision=HIGHEST) * window
        pairs.append((forward, backward))
    return pairs


def general_local(
    tokens,
    norm_gain,
    first_gate,
    second_gate,
    value_weight,
    short_weight,
    short_bias,
    embed_weight,
    embed_bias,
    inner_weight,
    inner_bias,
    filter_freq,
    filter_weight,
    filter_skip,
    output_gain,
    output_weight,
):
    row_count = lax.axis_size("row")
    row_index = lax.axis_index("row")
    col_index = lax.axis_index("col")
    local_tokens = tokens.shape[0]
    length = local_tokens * row_count
    col_width = first_gate.shape[1]
    own_width = col_width // row_count
    widened = tokens.astype(jnp.float32)
    normed = (
        widened
        * lax.rsqrt(jnp.mean(widened * widened, axis=1, keepdims=True) + NORM_EPS)
        * norm_gain
    ).astype(jnp.bfloat16)
    gate_first = jnp.dot(normed, first_gate, preferred_element_type=jnp.float32).astype(
        jnp.bfloat16
    )
    gate_second = jnp.dot(normed, second_gate, preferred_element_type=jnp.float32).astype(
        jnp.bfloat16
    )
    gate_value = jnp.dot(normed, value_weight, preferred_element_type=jnp.float32).astype(
        jnp.bfloat16
    )
    position_ramp, hidden = filter_hidden(
        length, embed_weight, embed_bias, inner_weight, inner_bias, filter_freq
    )
    channel_start = (col_index * row_count + row_index) * own_width
    deltas = lax.dynamic_slice_in_dim(decay_rates(), channel_start, own_width)
    tap_pairs = channel_taps(hidden, position_ramp, filter_weight, deltas)
    tables = make_tables(2 * length)
    half_width = short_weight.shape[1] // 2
    moved = (
        lax.all_to_all(gate_first, "row", split_axis=1, concat_axis=0, tiled=True),
        lax.all_to_all(gate_second, "row", split_axis=1, concat_axis=0, tiled=True),
        lax.all_to_all(gate_value, "row", split_axis=1, concat_axis=0, tiled=True),
    )
    weights_own = lax.dynamic_slice_in_dim(short_weight, row_index * own_width, own_width, 2)
    bias_own = lax.dynamic_slice_in_dim(short_bias, row_index * own_width, own_width, 1)
    smoothed = [
        short_filter(
            jnp.pad(moved[branch], ((half_width, half_width), (0, 0))),
            weights_own[branch],
            bias_own[branch],
            length,
        )
        for branch in range(3)
    ]
    signal = smoothed[2]
    for order_index in range(2):
        signal = smoothed[order_index] * two_sided(
            signal,
            tap_pairs[order_index][0],
            tap_pairs[order_index][1],
            filter_skip[order_index],
            tables,
        )
    result = jax.tree.map(
        lambda part, own: part.astype(own.dtype),
        lax.all_to_all(for_sending(signal), "row", split_axis=0, concat_axis=1, tiled=True),
        signal,
    )
    group_width = CHANNELS // GROUPS
    grouped = result.reshape(local_tokens, col_width // group_width, group_width)
    scaled = grouped * lax.rsqrt(jnp.mean(grouped * grouped, axis=2, keepdims=True) + NORM_EPS)
    mix_local = (scaled.reshape(local_tokens, col_width) * output_gain).astype(jnp.bfloat16)
    gathered = lax.all_to_all(mix_local, "col", split_axis=0, concat_axis=1, tiled=True)
    return jnp.dot(gathered, output_weight, preferred_element_type=jnp.float32).astype(jnp.bfloat16)


LANES = 128
SUBLANES = 16
BF16 = jnp.bfloat16
F32 = jnp.float32


def fast_tables(length, rows, tile_rows, own):
    total = 2 * length
    majors = length // LANES
    n1 = (np.arange(rows)[None, :] * tile_rows + np.arange(tile_rows)[:, None]).reshape(-1)
    k1 = np.arange(majors) + 0.5
    angle = 2.0 * np.pi * np.outer(k1, n1) / (2 * majors)
    eye = np.eye(own)
    inner = np.concatenate([np.kron(np.cos(angle), eye), np.kron(-np.sin(angle), eye)], 0)
    inner_back = inner.T * (2.0 / total)
    n2 = np.arange(LANES)
    turn = np.repeat(2.0 * np.pi * np.outer(k1, n2) / total, own, axis=0)
    twiddle = np.stack([np.cos(turn), np.sin(turn)])
    phase = 2.0 * np.pi * (np.outer(n2, n2) % LANES) / LANES
    c, s = np.cos(phase), np.sin(phase)
    outer = np.block([[c, -s], [s, c]])
    ramp = np.linspace(0.0, 1.0, length)
    angles = 2.0 * np.pi * np.arange(length) / length
    bands = np.linspace(0.0001, FREQ_BANDS - 1, FREQ_BANDS)[:, None]
    feats = np.concatenate([ramp[None], np.cos(bands * angles), -np.sin(bands * angles)], 0)
    return (
        jnp.asarray(inner, BF16),
        jnp.asarray(inner_back, BF16),
        jnp.asarray(twiddle, F32),
        jnp.asarray(outer, BF16),
        jnp.asarray(outer.T, BF16),
        jnp.asarray(feats, F32),
    )


def bounded_sin(x):
    turns = jnp.round(x * (1.0 / math.pi))
    r = x - turns * 3.140625
    r = r - turns * 9.67502593994140625e-4
    r = r - turns * 1.509957990978376432e-7
    half = turns * 0.5
    sign = 1.0 - 4.0 * (half - jnp.floor(half))
    q = r * r
    p = -2.5052108385e-8 + q * 1.6059043837e-10
    p = 2.7557319224e-6 + q * p
    p = -1.9841269841e-4 + q * p
    p = 8.3333333333e-3 + q * p
    p = -1.6666666667e-1 + q * p
    return sign * (r + r * q * p)


def mm(a, b):
    return jnp.dot(a.astype(BF16), b.astype(BF16), preferred_element_type=F32)


def tdot(a, b):
    return lax.dot_general(
        a, b, (((0,), (0,)), ((), ())), precision=HIGHEST, preferred_element_type=F32
    )


def column(row, start, count):
    shape = (count, row.shape[1])
    hit = lax.broadcasted_iota(jnp.int32, shape, 1) == start + lax.broadcasted_iota(
        jnp.int32, shape, 0
    )
    return jnp.sum(jnp.where(hit, row.astype(F32), 0.0), axis=1, keepdims=True)


def fast_kernel(
    dims,
    tokens_h,
    norm_gain,
    first_h,
    second_h,
    value_h,
    short_weight,
    short_bias,
    embed_weight,
    embed_bias,
    inner_weight,
    inner_bias,
    filter_freq,
    filter_weight,
    filter_skip,
    output_gain,
    out_w_h,
    inner_h,
    inner_back_h,
    twiddle_h,
    outer_h,
    outer_back_h,
    feats_h,
    out_ref,
    tokens_v,
    gates_v,
    out_w_v,
    inner_v,
    inner_back_v,
    twiddle_v,
    outer_v,
    outer_back_v,
    feats_v,
    normed_v,
    send_a,
    recv_a,
    send_b,
    recv_b,
    gains,
    gain_map,
    spectra,
    load_sem,
    send_a_sem,
    recv_a_sem,
    send_b_sem,
    recv_b_sem,
    send_g_sem,
    recv_g_sem,
):
    rows_n, cols_n, block, own = dims
    length = rows_n * block
    tiles = block // LANES
    piece = block // cols_n
    groups = LANES // piece
    half = own // groups
    row_me = lax.axis_index("row")
    col_me = lax.axis_index("col")
    me = row_me * cols_n + col_me
    everyone = rows_n * cols_n

    loads = [
        (tokens_h, tokens_v),
        (value_h, gates_v.at[2]),
        (first_h, gates_v.at[0]),
        (second_h, gates_v.at[1]),
        (feats_h, feats_v),
        (inner_h, inner_v),
        (twiddle_h, twiddle_v),
        (outer_h, outer_v),
        (outer_back_h, outer_back_v),
        (inner_back_h, inner_back_v),
    ] + [(out_w_h.at[:, g], out_w_v.at[g]) for g in range(groups)]
    copies = [
        pltpu.make_async_copy(src, dst, load_sem.at[i]) for i, (src, dst) in enumerate(loads)
    ]
    for copy in copies:
        copy.start()

    def place(flat):
        return (lax.div(flat, cols_n), lax.rem(flat, cols_n))

    barrier = pltpu.get_barrier_semaphore()
    for step in range(1, everyone):
        pl.semaphore_signal(
            barrier,
            inc=1,
            device_id=place(lax.rem(me + step, everyone)),
            device_id_type=pl.DeviceIdType.MESH,
        )

    copies[0].wait()
    gain_row = norm_gain[...]
    chunk = 32
    for start in range(0, block, chunk):
        x = tokens_v[start : start + chunk, :].astype(F32)
        scale = lax.rsqrt(jnp.mean(x * x, axis=1, keepdims=True) + NORM_EPS)
        normed_v[start : start + chunk, :] = (x * scale * gain_row).astype(BF16)

    sends = []
    for order, branch in enumerate((2, 0, 1)):
        copies[1 + order].wait()
        gate = jnp.dot(normed_v[...], gates_v[branch], preferred_element_type=F32)
        send_a[branch] = gate.T.astype(BF16).reshape(rows_n, own, block)
        if order == 0:
            pl.semaphore_wait(barrier, everyone - 1)
        for step in range(1, rows_n):
            peer = lax.rem(row_me + step, rows_n)
            copy = pltpu.make_async_remote_copy(
                src_ref=send_a.at[branch, peer],
                dst_ref=recv_a.at[branch, row_me],
                send_sem=send_a_sem.at[branch, step],
                recv_sem=recv_a_sem.at[branch, step],
                device_id=(peer, col_me),
                device_id_type=pl.DeviceIdType.MESH,
            )
            copy.start()
            sends.append((branch, copy))
        recv_a[branch, row_me] = send_a[branch, row_me]

    gain_sends = []
    gains[col_me] = output_gain[...]
    for step in range(1, cols_n):
        copy = pltpu.make_async_remote_copy(
            src_ref=output_gain,
            dst_ref=gains.at[col_me],
            send_sem=send_g_sem.at[step],
            recv_sem=recv_g_sem.at[step],
            device_id=(row_me, lax.rem(col_me + step, cols_n)),
            device_id_type=pl.DeviceIdType.MESH,
        )
        copy.start()
        gain_sends.append(copy)

    def to_layout(x):
        return jnp.concatenate(
            [
                jnp.concatenate(
                    [
                        x[:, g * half : (g + 1) * half, j * LANES : (j + 1) * LANES].reshape(
                            rows_n * half, LANES
                        )
                        for g in range(groups)
                    ],
                    axis=1,
                )
                for j in range(tiles)
            ],
            axis=0,
        )

    def taps_layout(x):
        return jnp.concatenate(
            [
                jnp.concatenate(
                    [
                        x[
                            g * half : (g + 1) * half,
                            (r * tiles + j) * LANES : (r * tiles + j + 1) * LANES,
                        ]
                        for g in range(groups)
                    ],
                    axis=1,
                )
                for j in range(tiles)
                for r in range(rows_n)
            ],
            axis=0,
        )

    freq = column(filter_freq[...], 0, filter_freq.shape[1])
    copies[4].wait()
    hidden = bounded_sin(
        freq
        * (
            tdot(embed_weight[...], feats_v[...])
            + column(embed_bias[...], 0, embed_bias.shape[1])
        )
    )
    hidden = bounded_sin(
        freq * (tdot(inner_weight[...], hidden) + column(inner_bias[...], 0, inner_bias.shape[1]))
    )
    channels = rows_n * cols_n * own
    slowest = math.log(DECAY_TARGET) / SLOW_SPAN
    fastest = math.log(DECAY_TARGET) / FAST_SPAN
    channel = (
        (col_me * rows_n + row_me) * own + lax.broadcasted_iota(jnp.int32, (own, 1), 0)
    ).astype(F32)
    decay = jnp.abs(slowest + channel * ((fastest - slowest) / (channels - 1)))
    lag = lax.broadcasted_iota(jnp.int32, (own, length), 1)
    window = jnp.exp(-(lag.astype(F32) * (1.0 / (length - 1))) * decay)
    for copy in copies[5:8]:
        copy.wait()

    def twist(real, imag, sign):
        cos = jnp.concatenate([twiddle_v[0]] * groups, axis=1)
        sin = jnp.concatenate([twiddle_v[1]] * groups, axis=1) * sign
        return real * cos + imag * sin, imag * cos - real * sin

    def lanes_of(x, g):
        return x[:, g * LANES : (g + 1) * LANES]

    def forward_inner(x):
        part = mm(inner_v[...], x)
        count = part.shape[0] // 2
        return twist(part[:count], part[count:], 1.0)

    for order in range(2):
        fwd = tdot(filter_weight[order, 0], hidden) * window
        bwd = jnp.where(lag == 0, 0.0, tdot(filter_weight[order, 1], hidden) * window)
        plus = forward_inner(taps_layout(fwd + bwd))
        minus = forward_inner(taps_layout(fwd - bwd))
        for g in range(groups):
            p = jnp.concatenate([lanes_of(plus[0], g), lanes_of(plus[1], g)], axis=1)
            m = jnp.concatenate([lanes_of(minus[0], g), lanes_of(minus[1], g)], axis=1)
            spectra[order, g, :, :LANES] = mm(p, outer_v[:, :LANES])
            spectra[order, g, :, LANES:] = mm(m, outer_v[:, LANES:])

    for copy in gain_sends:
        copy.wait_recv()
    lane = lax.broadcasted_iota(jnp.int32, (rows_n * half, LANES), 1)
    width = rows_n * own
    for q in range(cols_n):
        col_gain = column(gains[q], 0, width).reshape(rows_n, own, 1)
        result = jnp.zeros((rows_n * half, LANES), F32)
        for g in range(groups):
            part = col_gain[:, g * half : (g + 1) * half].reshape(rows_n * half, 1)
            result = jnp.where(lax.div(lane, piece) == g, part, result)
        gain_map[q] = result

    for copy in copies[8:10]:
        copy.wait()
    pos = lax.broadcasted_iota(jnp.int32, (rows_n, own, block), 2)

    def smooth(branch):
        for b, copy in sends:
            if b == branch:
                copy.wait_recv()
        x = recv_a[branch].astype(F32)
        flat = x.reshape(rows_n * own, block)
        before = pltpu.roll(flat, 1, 1).reshape(rows_n, own, block)
        after = pltpu.roll(flat, block - 1, 1).reshape(rows_n, own, block)
        gap = jnp.zeros((1, own, block), F32)
        before = jnp.where(pos == 0, jnp.concatenate([gap, before[:-1]], 0), before)
        after = jnp.where(pos == block - 1, jnp.concatenate([after[1:], gap], 0), after)
        start = row_me * own
        w = [
            column(short_weight[branch, j : j + 1, :], start, own).reshape(1, own, 1)
            for j in range(3)
        ]
        bias = column(short_bias[branch : branch + 1, :], start, own).reshape(1, own, 1)
        return to_layout(bias + before * w[0] + x * w[1] + after * w[2])

    signal = smooth(2)
    for order in range(2):
        real, imag = forward_inner(signal)
        back_real, back_imag = [], []
        for g in range(groups):
            t = jnp.concatenate([lanes_of(real, g), lanes_of(imag, g)], axis=1)
            spec = mm(t, outer_v[...])
            sr, si = spec[:, :LANES], spec[:, LANES:]
            hr, hi = spectra[order, g, :, :LANES], spectra[order, g, :, LANES:]
            prod = jnp.concatenate([sr * hr - si * hi, sr * hi + si * hr], axis=1)
            back = mm(prod, outer_back_v[...])
            back_real.append(back[:, :LANES])
            back_imag.append(back[:, LANES:])
        ur, ui = twist(jnp.concatenate(back_real, 1), jnp.concatenate(back_imag, 1), -1.0)
        conv = mm(inner_back_v[...], jnp.concatenate([ur, ui], axis=0))
        skip = column(filter_skip[order : order + 1, :], 0, own)
        skip = to_layout(jnp.broadcast_to(skip[None], (rows_n, own, block)))
        signal = smooth(order) * (conv + signal * skip)

    count = rows_n * half
    for j in range(tiles):
        for h in range(LANES // piece):
            part = jnp.concatenate(
                [
                    signal[
                        j * count : (j + 1) * count,
                        g * LANES + h * piece : g * LANES + (h + 1) * piece,
                    ]
                    for g in range(groups)
                ],
                axis=1,
            )
            send_b[j * (LANES // piece) + h] = part.astype(BF16).reshape(rows_n, half, LANES)
    last = []
    for step in range(1, everyone):
        row_to, col_to = place(lax.rem(me + step, everyone))
        copy = pltpu.make_async_remote_copy(
            src_ref=send_b.at[col_to, row_to],
            dst_ref=recv_b.at[col_me, row_me],
            send_sem=send_b_sem.at[step],
            recv_sem=recv_b_sem.at[step],
            device_id=(row_to, col_to),
            device_id_type=pl.DeviceIdType.MESH,
        )
        copy.start()
        last.append(copy)
    recv_b[col_me, row_me] = send_b[col_me, row_me]
    for copy in copies[10:]:
        copy.wait()
    for copy in last:
        copy.wait_recv()

    group_width = CHANNELS // GROUPS
    per_group = group_width // own
    turned = []
    for q in range(cols_n):
        for r in range(0, rows_n, per_group):
            x = recv_b[q, r : r + per_group].astype(F32).reshape(per_group * half, LANES)
            total = jnp.sum(x * x, axis=0, keepdims=True)
            square = total
            for g in range(1, groups):
                square = square + pltpu.roll(total, g * piece, 1)
            scale = lax.rsqrt(square * (1.0 / group_width) + NORM_EPS)
            gain = gain_map[q, r * half : (r + per_group) * half, :]
            turned.append(x * scale * gain)
    mixed = jnp.concatenate(turned, axis=0).T.astype(BF16)
    depth = everyone * half
    step_width = 512
    for start in range(0, out_ref.shape[1], step_width):
        acc = jnp.zeros((piece, step_width), F32)
        for g in range(groups):
            acc = acc + jnp.dot(
                mixed[g * piece : (g + 1) * piece],
                out_w_v[g, :, :, start : start + step_width].reshape(depth, step_width),
                preferred_element_type=F32,
            )
        out_ref[:, start : start + step_width] = acc.astype(BF16)

    for _, copy in sends:
        copy.wait_send()
    for copy in gain_sends + last:
        copy.wait_send()


def fast_local(*args):
    (
        tokens, norm_gain, first_gate, second_gate, value_weight, short_weight, short_bias,
        embed_weight, embed_bias, inner_weight, inner_bias, filter_freq, filter_weight,
        filter_skip, output_gain, output_weight,
    ) = args
    rows_n, cols_n = lax.axis_size("row"), lax.axis_size("col")
    block, model = tokens.shape
    own = filter_weight.shape[3]
    piece = block // cols_n
    groups = LANES // piece
    half = own // groups
    tiles = block // LANES
    length = block * rows_n
    width = first_gate.shape[1]
    everyone = rows_n * cols_n
    tables = fast_tables(length, rows_n, tiles, half)
    out_width = output_weight.shape[1]
    out_w = output_weight.reshape(everyone, groups, half, out_width)
    vm = pl.BlockSpec(memory_space=pltpu.VMEM)
    hbm = pl.BlockSpec(memory_space=pl.ANY)
    operands = [
        (tokens, hbm),
        (norm_gain.reshape(1, -1), vm),
        (first_gate, hbm),
        (second_gate, hbm),
        (value_weight, hbm),
        (short_weight, vm),
        (short_bias, vm),
        (embed_weight, vm),
        (embed_bias.reshape(1, -1), vm),
        (inner_weight, vm),
        (inner_bias.reshape(1, -1), vm),
        (filter_freq.reshape(1, -1), vm),
        (filter_weight, vm),
        (filter_skip, vm),
        (output_gain.reshape(1, -1), vm),
        (out_w, hbm),
    ] + [(table, hbm) for table in tables]
    rows_all = tiles * rows_n * half
    DMA = pltpu.SemaphoreType.DMA
    return pl.pallas_call(
        functools.partial(fast_kernel, (rows_n, cols_n, block, own)),
        out_shape=jax.ShapeDtypeStruct((piece, out_width), BF16),
        in_specs=[spec for _, spec in operands],
        out_specs=vm,
        scratch_shapes=[
            pltpu.VMEM(tokens.shape, BF16),
            pltpu.VMEM((3, model, width), BF16),
            pltpu.VMEM((groups, everyone, half, out_width), BF16),
        ]
        + [pltpu.VMEM(table.shape, table.dtype) for table in tables]
        + [
            pltpu.VMEM(tokens.shape, BF16),
            pltpu.VMEM((3, rows_n, own, block), BF16),
            pltpu.VMEM((3, rows_n, own, block), BF16),
            pltpu.VMEM((cols_n, rows_n, half, LANES), BF16),
            pltpu.VMEM((cols_n, rows_n, half, LANES), BF16),
            pltpu.VMEM((cols_n, 1, width), F32),
            pltpu.VMEM((cols_n, rows_n * half, LANES), F32),
            pltpu.VMEM((2, groups, rows_all, 2 * LANES), F32),
            DMA((10 + groups,)),
            DMA((3, rows_n)),
            DMA((3, rows_n)),
            DMA((everyone,)),
            DMA((everyone,)),
            DMA((cols_n,)),
            DMA((cols_n,)),
        ],
        compiler_params=pltpu.CompilerParams(
            collective_id=0, has_side_effects=True, vmem_limit_bytes=56 * 1024 * 1024
        ),
    )(*[operand for operand, _ in operands])


def kernel_fits(tokens, filter_weight, rows_n, cols_n):
    block = tokens.shape[0]
    own = filter_weight.shape[3]
    piece = block // cols_n
    if block % LANES or LANES % piece:
        return False
    groups = LANES // piece
    return own % (groups * SUBLANES) == 0 and (CHANNELS // GROUPS) % own == 0


def local(*args):
    if kernel_fits(args[0], args[12], lax.axis_size("row"), lax.axis_size("col")):
        return fast_local(*args)
    return general_local(*args)


def solution(mesh):
    in_specs = (
        P("row", None),
        P(),
        P(None, "col"),
        P(None, "col"),
        P(None, "col"),
        P(None, None, "col"),
        P(None, "col"),
        P(),
        P(),
        P(),
        P(),
        P(),
        P(None, None, None, ("col", "row")),
        P(None, ("col", "row")),
        P("col"),
        P(),
    )
    out_specs = P(("row", "col"), None)
    return jax.shard_map(local, mesh=mesh, in_specs=in_specs, out_specs=out_specs, check_vma=False)
```

profile of v0, /device:TPU:0, one launch (start us, length us, event | category | flops | bytes accessed | tf_op | source)
XLA Modules:
  0.0 29.6 jit_solution(10955744754281147945)
XLA Ops:
  0.0 1.6 %copy.23.filter_weight = f32[2,2,64,32]{3,2,1,0:T(8,128)} copy(f32[2,2,64,32]{2,3,1,0:T(8,128)} %param.34) | data formatting | bytes 65536 | tf_op args[12]
  1.6 26.3 %shard_map.208 = bf16[64,2048]{1,0:T(8,128)(2,1)} custom-call(bf16[256,2048]{1,0:T(8,128)(2,1)} %tokens_h.1, f32[1,2048]{1,0:T(1,128)} %bitcast.7, bf16[2048,256]{1,0:T(8,128)(2,1)} %first_h.1, bf16[2048,256]{1,0:T(8,128)(2,1)} %second_h.1, bf16[2048,256]{1,0:T(8,128)(2,1)} %value_h.1, bf16[3,3,256]{2,1,0:T(4,128)(2,1)} %short_weight.1, ...), custom_call_target="tpu_custom_call" | custom-call | tf_op jit(solution)/shard_map/pallas_call | solution.py:709
  27.9 1.7 %copy.25 = bf16[64,2048]{1,0:T(8,128)(2,1)} copy(bf16[64,2048]{1,0:T(8,128)(2,1)} %shard_map.208) | data formatting | bytes 524288
where the time goes:
time: 29.8 us; the launch traced here: 29.6 us
  Pallas kernels  26.3 us (88%)
  local copies, waits for them, and re-layouts  3.26 us (11%)
    pallas_call x1, Pallas kernels, fast_local(): pl.pallas_call(functools.partial(fast_kernel, (rows_n, cols_n, block, own...  26.3 us
    unnamed x2, local copies, waits for them, and re-layouts  3.26 us

commit v1 on v0

--- a/solution.py
+++ b/solution.py
@@ -320,6 +320,10 @@
     )
 
 
+def fdot(a, b):
+    return jnp.dot(a, b, precision=HIGHEST, preferred_element_type=F32)
+
+
 def column(row, start, count):
     shape = (count, row.shape[1])
     hit = lax.broadcasted_iota(jnp.int32, shape, 1) == start + lax.broadcasted_iota(
@@ -328,56 +332,27 @@
     return jnp.sum(jnp.where(hit, row.astype(F32), 0.0), axis=1, keepdims=True)
 
 
-def fast_kernel(
-    dims,
-    tokens_h,
-    norm_gain,
-    first_h,
-    second_h,
-    value_h,
-    short_weight,
-    short_bias,
-    embed_weight,
-    embed_bias,
-    inner_weight,
-    inner_bias,
-    filter_freq,
-    filter_weight,
-    filter_skip,
-    output_gain,
-    out_w_h,
-    inner_h,
-    inner_back_h,
-    twiddle_h,
-    outer_h,
-    outer_back_h,
-    feats_h,
-    out_ref,
-    tokens_v,
-    gates_v,
-    out_w_v,
-    inner_v,
-    inner_back_v,
-    twiddle_v,
-    outer_v,
-    outer_back_v,
-    feats_v,
-    normed_v,
-    send_a,
-    recv_a,
-    send_b,
-    recv_b,
-    gains,
-    gain_map,
-    spectra,
-    load_sem,
-    send_a_sem,
-    recv_a_sem,
-    send_b_sem,
-    recv_b_sem,
-    send_g_sem,
-    recv_g_sem,
-):
+SMALL = 11
+
+
+def fast_kernel(dims, *refs):
+    tokens_h, first_h, second_h, value_h, out_w_h = refs[:5]
+    small_h = refs[5 : 5 + SMALL]
+    inner_h, inner_back_h, twiddle_h, outer_h, outer_back_h, feats_h, out_ref = refs[
+        5 + SMALL : 12 + SMALL
+    ]
+    tokens_v, gates_v, out_w_v = refs[12 + SMALL : 15 + SMALL]
+    small_v = refs[15 + SMALL : 15 + 2 * SMALL]
+    (
+        norm_gain, short_weight, short_bias, embed_weight, embed_bias, inner_weight,
+        inner_bias, filter_freq, filter_weight, filter_skip, output_gain,
+    ) = small_v
+    (
+        inner_v, inner_back_v, twiddle_v, outer_v, outer_back_v, feats_v, normed_v,
+        send_a, recv_a, send_b, recv_b, send_s, recv_s, second_v, send_h, recv_h, gains,
+        gain_map, spectra, load_sem, small_sem, send_a_sem, recv_a_sem, send_b_sem,
+        recv_b_sem, send_g_sem, recv_g_sem, send_s_sem, recv_s_sem, send_h_sem, recv_h_sem,
+    ) = refs[15 + 2 * SMALL :]
     rows_n, cols_n, block, own = dims
     length = rows_n * block
     tiles = block // LANES
@@ -404,8 +379,13 @@
     copies = [
         pltpu.make_async_copy(src, dst, load_sem.at[i]) for i, (src, dst) in enumerate(loads)
     ]
-    for copy in copies:
-        copy.start()
+    smalls = [
+        pltpu.make_async_copy(src, dst, small_sem.at[i])
+        for i, (src, dst) in enumerate(zip(small_h, small_v))
+    ]
+    copies[0].start()
+    smalls[0].start()
+    copies[1].start()
 
     def place(flat):
         return (lax.div(flat, cols_n), lax.rem(flat, cols_n))
@@ -419,7 +399,10 @@
             device_id_type=pl.DeviceIdType.MESH,
         )
 
+    for copy in copies[2:10] + smalls[1:]:
+        copy.start()
     copies[0].wait()
+    smalls[0].wait()
     gain_row = norm_gain[...]
     chunk = 32
     for start in range(0, block, chunk):
@@ -427,26 +410,50 @@
         scale = lax.rsqrt(jnp.mean(x * x, axis=1, keepdims=True) + NORM_EPS)
         normed_v[start : start + chunk, :] = (x * scale * gain_row).astype(BF16)
 
+    MESH = pl.DeviceIdType.MESH
     sends = []
-    for order, branch in enumerate((2, 0, 1)):
+    for order, branch in enumerate((2, 0)):
         copies[1 + order].wait()
         gate = jnp.dot(normed_v[...], gates_v[branch], preferred_element_type=F32)
-        send_a[branch] = gate.T.astype(BF16).reshape(rows_n, own, block)
+        send_a[order] = gate.T.astype(BF16).reshape(rows_n, own, block)
         if order == 0:
             pl.semaphore_wait(barrier, everyone - 1)
         for step in range(1, rows_n):
             peer = lax.rem(row_me + step, rows_n)
             copy = pltpu.make_async_remote_copy(
-                src_ref=send_a.at[branch, peer],
-                dst_ref=recv_a.at[branch, row_me],
-                send_sem=send_a_sem.at[branch, step],
-                recv_sem=recv_a_sem.at[branch, step],
+                src_ref=send_a.at[order, peer],
+                dst_ref=recv_a.at[order, row_me],
+                send_sem=send_a_sem.at[order, step],
+                recv_sem=recv_a_sem.at[order, step],
                 device_id=(peer, col_me),
-                device_id_type=pl.DeviceIdType.MESH,
+                device_id_type=MESH,
             )
             copy.start()
-            sends.append((branch, copy))
-        recv_a[branch, row_me] = send_a[branch, row_me]
+            sends.append((order, copy))
+        recv_a[order, row_me] = send_a[order, row_me]
+
+    for copy in copies[10:]:
+        copy.start()
+    copies[3].wait()
+    gate = jnp.dot(normed_v[...], gates_v[1], preferred_element_type=F32)
+    gate = gate.astype(BF16).astype(F32)
+    second_v[...] = gate.T
+    send_h[0] = gate[:1]
+    send_h[1] = gate[block - 1 :]
+    halo_sends = []
+    for edge, shift in ((0, rows_n - 1), (1, 1)):
+        copy = pltpu.make_async_remote_copy(
+            src_ref=send_h.at[edge],
+            dst_ref=recv_h.at[edge],
+            send_sem=send_h_sem.at[edge],
+            recv_sem=recv_h_sem.at[edge],
+            device_id=(lax.rem(row_me + shift, rows_n), col_me),
+            device_id_type=MESH,
+        )
+        copy.start()
+        halo_sends.append(copy)
+    for copy in smalls[1:]:
+        copy.wait()
 
     gain_sends = []
     gains[col_me] = output_gain[...]
@@ -536,8 +543,8 @@
         return twist(part[:count], part[count:], 1.0)
 
     for order in range(2):
-        fwd = tdot(filter_weight[order, 0], hidden) * window
-        bwd = jnp.where(lag == 0, 0.0, tdot(filter_weight[order, 1], hidden) * window)
+        fwd = fdot(filter_weight[order, 0], hidden) * window
+        bwd = jnp.where(lag == 0, 0.0, fdot(filter_weight[order, 1], hidden) * window)
         plus = forward_inner(taps_layout(fwd + bwd))
         minus = forward_inner(taps_layout(fwd - bwd))
         for g in range(groups):
@@ -546,10 +553,43 @@
             spectra[order, g, :, :LANES] = mm(p, outer_v[:, :LANES])
             spectra[order, g, :, LANES:] = mm(m, outer_v[:, LANES:])
 
+    for copy in halo_sends:
+        copy.wait_recv()
+    width = rows_n * own
+    count = rows_n * half
+    x = second_v[...]
+    spot = lax.broadcasted_iota(jnp.int32, (width, block), 1)
+    first_col = jnp.where(row_me == 0, 0.0, column(recv_h[1], 0, width))
+    last_col = jnp.where(row_me == rows_n - 1, 0.0, column(recv_h[0], 0, width))
+    before = jnp.where(spot == 0, first_col, pltpu.roll(x, 1, 1))
+    after = jnp.where(spot == block - 1, last_col, pltpu.roll(x, block - 1, 1))
+    w = [column(short_weight[1, j : j + 1, :], 0, width) for j in range(3)]
+    x = column(short_bias[1:2, :], 0, width) + before * w[0] + x * w[1] + after * w[2]
+    x = x.reshape(rows_n, groups, half, block)
+    for q in range(cols_n):
+        part = jnp.concatenate(
+            [x[:, g, :, q * piece : (q + 1) * piece].reshape(count, piece) for g in range(groups)],
+            axis=1,
+        )
+        send_s[q] = part.astype(BF16)
+    recv_s[col_me] = send_s[col_me]
+    second_sends = []
+    for step in range(1, cols_n):
+        peer = lax.rem(col_me + step, cols_n)
+        copy = pltpu.make_async_remote_copy(
+            src_ref=send_s.at[peer],
+            dst_ref=recv_s.at[col_me],
+            send_sem=send_s_sem.at[step],
+            recv_sem=recv_s_sem.at[step],
+            device_id=(row_me, peer),
+            device_id_type=MESH,
+        )
+        copy.start()
+        second_sends.append(copy)
+
     for copy in gain_sends:
         copy.wait_recv()
     lane = lax.broadcasted_iota(jnp.int32, (rows_n * half, LANES), 1)
-    width = rows_n * own
     for q in range(cols_n):
         col_gain = column(gains[q], 0, width).reshape(rows_n, own, 1)
         result = jnp.zeros((rows_n * half, LANES), F32)
@@ -562,11 +602,11 @@
         copy.wait()
     pos = lax.broadcasted_iota(jnp.int32, (rows_n, own, block), 2)
 
-    def smooth(branch):
+    def smooth(slot, branch):
         for b, copy in sends:
-            if b == branch:
+            if b == slot:
                 copy.wait_recv()
-        x = recv_a[branch].astype(F32)
+        x = recv_a[slot].astype(F32)
         flat = x.reshape(rows_n * own, block)
         before = pltpu.roll(flat, 1, 1).reshape(rows_n, own, block)
         after = pltpu.roll(flat, block - 1, 1).reshape(rows_n, own, block)
@@ -581,7 +621,7 @@
         bias = column(short_bias[branch : branch + 1, :], start, own).reshape(1, own, 1)
         return to_layout(bias + before * w[0] + x * w[1] + after * w[2])
 
-    signal = smooth(2)
+    signal = smooth(0, 2)
     for order in range(2):
         real, imag = forward_inner(signal)
         back_real, back_imag = [], []
@@ -598,9 +638,10 @@
         conv = mm(inner_back_v[...], jnp.concatenate([ur, ui], axis=0))
         skip = column(filter_skip[order : order + 1, :], 0, own)
         skip = to_layout(jnp.broadcast_to(skip[None], (rows_n, own, block)))
-        signal = smooth(order) * (conv + signal * skip)
-
-    count = rows_n * half
+        signal = conv + signal * skip
+        if order == 0:
+            signal = signal * smooth(1, 0)
+
     for j in range(tiles):
         for h in range(LANES // piece):
             part = jnp.concatenate(
@@ -630,7 +671,7 @@
     recv_b[col_me, row_me] = send_b[col_me, row_me]
     for copy in copies[10:]:
         copy.wait()
-    for copy in last:
+    for copy in second_sends + last:
         copy.wait_recv()
 
     group_width = CHANNELS // GROUPS
@@ -639,6 +680,7 @@
     for q in range(cols_n):
         for r in range(0, rows_n, per_group):
             x = recv_b[q, r : r + per_group].astype(F32).reshape(per_group * half, LANES)
+            x = x * recv_s[q, r * half : (r + per_group) * half, :].astype(F32)
             total = jnp.sum(x * x, axis=0, keepdims=True)
             square = total
             for g in range(1, groups):
@@ -661,7 +703,7 @@
 
     for _, copy in sends:
         copy.wait_send()
-    for copy in gain_sends + last:
+    for copy in halo_sends + gain_sends + second_sends + last:
         copy.wait_send()
 
 
@@ -686,58 +728,64 @@
     out_w = output_weight.reshape(everyone, groups, half, out_width)
     vm = pl.BlockSpec(memory_space=pltpu.VMEM)
     hbm = pl.BlockSpec(memory_space=pl.ANY)
-    operands = [
-        (tokens, hbm),
-        (norm_gain.reshape(1, -1), vm),
-        (first_gate, hbm),
-        (second_gate, hbm),
-        (value_weight, hbm),
-        (short_weight, vm),
-        (short_bias, vm),
-        (embed_weight, vm),
-        (embed_bias.reshape(1, -1), vm),
-        (inner_weight, vm),
-        (inner_bias.reshape(1, -1), vm),
-        (filter_freq.reshape(1, -1), vm),
-        (filter_weight, vm),
-        (filter_skip, vm),
-        (output_gain.reshape(1, -1), vm),
-        (out_w, hbm),
-    ] + [(table, hbm) for table in tables]
+    small = [
+        norm_gain.reshape(1, -1),
+        short_weight,
+        short_bias,
+        embed_weight,
+        embed_bias.reshape(1, -1),
+        inner_weight,
+        inner_bias.reshape(1, -1),
+        filter_freq.reshape(1, -1),
+        jnp.swapaxes(filter_weight, 2, 3),
+        filter_skip,
+        output_gain.reshape(1, -1),
+    ]
+    operands = [tokens, first_gate, second_gate, value_weight, out_w, *small, *tables]
     rows_all = tiles * rows_n * half
     DMA = pltpu.SemaphoreType.DMA
     return pl.pallas_call(
         functools.partial(fast_kernel, (rows_n, cols_n, block, own)),
         out_shape=jax.ShapeDtypeStruct((piece, out_width), BF16),
-        in_specs=[spec for _, spec in operands],
+        in_specs=[hbm] * len(operands),
         out_specs=vm,
         scratch_shapes=[
             pltpu.VMEM(tokens.shape, BF16),
             pltpu.VMEM((3, model, width), BF16),
             pltpu.VMEM((groups, everyone, half, out_width), BF16),
         ]
-        + [pltpu.VMEM(table.shape, table.dtype) for table in tables]
+        + [pltpu.VMEM(array.shape, array.dtype) for array in small + list(tables)]
         + [
             pltpu.VMEM(tokens.shape, BF16),
-            pltpu.VMEM((3, rows_n, own, block), BF16),
-            pltpu.VMEM((3, rows_n, own, block), BF16),
+            pltpu.VMEM((2, rows_n, own, block), BF16),
+            pltpu.VMEM((2, rows_n, own, block), BF16),
             pltpu.VMEM((cols_n, rows_n, half, LANES), BF16),
             pltpu.VMEM((cols_n, rows_n, half, LANES), BF16),
+            pltpu.VMEM((cols_n, rows_n * half, LANES), BF16),
+            pltpu.VMEM((cols_n, rows_n * half, LANES), BF16),
+            pltpu.VMEM((width, block), F32),
+            pltpu.VMEM((2, 1, width), F32),
+            pltpu.VMEM((2, 1, width), F32),
             pltpu.VMEM((cols_n, 1, width), F32),
             pltpu.VMEM((cols_n, rows_n * half, LANES), F32),
             pltpu.VMEM((2, groups, rows_all, 2 * LANES), F32),
             DMA((10 + groups,)),
-            DMA((3, rows_n)),
-            DMA((3, rows_n)),
+            DMA((SMALL,)),
+            DMA((2, rows_n)),
+            DMA((2, rows_n)),
             DMA((everyone,)),
             DMA((everyone,)),
             DMA((cols_n,)),
             DMA((cols_n,)),
+            DMA((cols_n,)),
+            DMA((cols_n,)),
+            DMA((2,)),
+            DMA((2,)),
         ],
         compiler_params=pltpu.CompilerParams(
             collective_id=0, has_side_effects=True, vmem_limit_bytes=56 * 1024 * 1024
         ),
-    )(*[operand for operand, _ in operands])
+    )(*operands)
 
 
 def kernel_fits(tokens, filter_weight, rows_n, cols_n):

time: 29.8 us -> 26.4 us (0.89)
  Pallas kernels: 26.3 us -> 24.6 us
  local copies, waits for them, and re-layouts: 3.26 us -> 1.67 us
    pallas_call x1, Pallas kernels: 26.3 us -> 24.6 us  [fast_local(): pl.pallas_call(functools.partial(fast_kernel, (rows_n, cols_n, block, own...]
    unnamed x2 -> x1, local copies, waits for them, and re-layouts: 3.26 us -> 1.67 us
where the time goes in v1:
time: 26.4 us; the launch traced here: 26.3 us
  Pallas kernels  24.6 us (93%)
  local copies, waits for them, and re-layouts  1.67 us (6%)
    pallas_call x1, Pallas kernels, fast_local(): pl.pallas_call(functools.partial(fast_kernel, (rows_n, cols_n, block, own...  24.6 us
    unnamed x1, local copies, waits for them, and re-layouts  1.67 us

profile of v1, /device:TPU:0, one launch (start us, length us, event | category | flops | bytes accessed | tf_op | source)
XLA Modules:
  0.0 26.3 jit_solution(15818623483942526161)
XLA Ops:
  0.0 24.6 %shard_map.208 = bf16[64,2048]{1,0:T(8,128)(2,1)} custom-call(bf16[256,2048]{1,0:T(8,128)(2,1)} %refs_0_.1, bf16[2048,256]{1,0:T(8,128)(2,1)} %refs_1_.1, bf16[2048,256]{1,0:T(8,128)(2,1)} %refs_2_.1, bf16[2048,256]{1,0:T(8,128)(2,1)} %refs_3_.1, bf16[32,2,16,2048]{3,2,1,0:T(8,128)(2,1)} %bitcast.7, f32[1,2048]{1,0:T(1,128)} %bitcast.9, ...), custom_call_target="tpu_custom_call" | custom-call | tf_op jit(solution)/shard_map/pallas_call | solution.py:747
  24.6 1.7 %copy.24 = bf16[64,2048]{1,0:T(8,128)(2,1)} copy(bf16[64,2048]{1,0:T(8,128)(2,1)} %shard_map.208) | data formatting | bytes 524288

commit v2 on v1

--- a/solution.py
+++ b/solution.py
@@ -284,13 +284,16 @@
     angles = 2.0 * np.pi * np.arange(length) / length
     bands = np.linspace(0.0001, FREQ_BANDS - 1, FREQ_BANDS)[:, None]
     feats = np.concatenate([ramp[None], np.cos(bands * angles), -np.sin(bands * angles)], 0)
+    feats = np.pad(feats, ((0, -feats.shape[0] % SUBLANES), (0, 0))).astype(np.float32)
+    high = feats.astype(BF16)
+    low = (feats - high.astype(np.float32)).astype(BF16)
     return (
         jnp.asarray(inner, BF16),
         jnp.asarray(inner_back, BF16),
         jnp.asarray(twiddle, F32),
         jnp.asarray(outer, BF16),
         jnp.asarray(outer.T, BF16),
-        jnp.asarray(feats, F32),
+        jnp.asarray(np.concatenate([high, low, high], 0)),
     )
 
 
@@ -314,14 +317,24 @@
     return jnp.dot(a.astype(BF16), b.astype(BF16), preferred_element_type=F32)
 
 
-def tdot(a, b):
+def halves(x):
+    high = x.astype(BF16).astype(F32)
+    return high, x - high
+
+
+def tdot(a, stacked):
+    high, low = halves(a)
     return lax.dot_general(
-        a, b, (((0,), (0,)), ((), ())), precision=HIGHEST, preferred_element_type=F32
-    )
-
-
-def fdot(a, b):
-    return jnp.dot(a, b, precision=HIGHEST, preferred_element_type=F32)
+        jnp.concatenate([high, high, low], 0).astype(BF16),
+        stacked,
+        (((0,), (0,)), ((), ())),
+        preferred_element_type=F32,
+    )
+
+
+def stack(b):
+    high, low = halves(b)
+    return jnp.concatenate([high, low, high], 0).astype(BF16)
 
 
 def column(row, start, count):
@@ -350,7 +363,7 @@
     (
         inner_v, inner_back_v, twiddle_v, outer_v, outer_back_v, feats_v, normed_v,
         send_a, recv_a, send_b, recv_b, send_s, recv_s, second_v, send_h, recv_h, gains,
-        gain_map, spectra, load_sem, small_sem, send_a_sem, recv_a_sem, send_b_sem,
+        gain_map, spectra, embed_pad, load_sem, small_sem, send_a_sem, recv_a_sem, send_b_sem,
         recv_b_sem, send_g_sem, recv_g_sem, send_s_sem, recv_s_sem, send_h_sem, recv_h_sem,
     ) = refs[15 + 2 * SMALL :]
     rows_n, cols_n, block, own = dims
@@ -367,8 +380,8 @@
     loads = [
         (tokens_h, tokens_v),
         (value_h, gates_v.at[2]),
+        (second_h, gates_v.at[1]),
         (first_h, gates_v.at[0]),
-        (second_h, gates_v.at[1]),
         (feats_h, feats_v),
         (inner_h, inner_v),
         (twiddle_h, twiddle_v),
@@ -412,8 +425,9 @@
 
     MESH = pl.DeviceIdType.MESH
     sends = []
-    for order, branch in enumerate((2, 0)):
-        copies[1 + order].wait()
+
+    def project(order, branch):
+        copies[1 + 2 * order].wait()
         gate = jnp.dot(normed_v[...], gates_v[branch], preferred_element_type=F32)
         send_a[order] = gate.T.astype(BF16).reshape(rows_n, own, block)
         if order == 0:
@@ -432,9 +446,8 @@
             sends.append((order, copy))
         recv_a[order, row_me] = send_a[order, row_me]
 
-    for copy in copies[10:]:
-        copy.start()
-    copies[3].wait()
+    project(0, 2)
+    copies[2].wait()
     gate = jnp.dot(normed_v[...], gates_v[1], preferred_element_type=F32)
     gate = gate.astype(BF16).astype(F32)
     second_v[...] = gate.T
@@ -452,6 +465,9 @@
         )
         copy.start()
         halo_sends.append(copy)
+    project(1, 0)
+    for copy in copies[10:]:
+        copy.start()
     for copy in smalls[1:]:
         copy.wait()
 
@@ -507,15 +523,17 @@
 
     freq = column(filter_freq[...], 0, filter_freq.shape[1])
     copies[4].wait()
+    embed_pad[...] = jnp.zeros_like(embed_pad)
+    embed_pad[: embed_weight.shape[0], :] = embed_weight[...]
     hidden = bounded_sin(
         freq
         * (
-            tdot(embed_weight[...], feats_v[...])
+            tdot(embed_pad[...], feats_v[...])
             + column(embed_bias[...], 0, embed_bias.shape[1])
         )
     )
     hidden = bounded_sin(
-        freq * (tdot(inner_weight[...], hidden) + column(inner_bias[...], 0, inner_bias.shape[1]))
+        freq * (tdot(inner_weight[...], stack(hidden)) + column(inner_bias[...], 0, inner_bias.shape[1]))
     )
     channels = rows_n * cols_n * own
     slowest = math.log(DECAY_TARGET) / SLOW_SPAN
@@ -542,9 +560,16 @@
         count = part.shape[0] // 2
         return twist(part[:count], part[count:], 1.0)
 
+    high, low = halves(filter_weight[...].reshape(4 * own, filter_weight.shape[3]))
+    taps = jnp.dot(
+        jnp.concatenate([high, high, low], 1).astype(BF16),
+        stack(hidden),
+        preferred_element_type=F32,
+    )
     for order in range(2):
-        fwd = fdot(filter_weight[order, 0], hidden) * window
-        bwd = jnp.where(lag == 0, 0.0, fdot(filter_weight[order, 1], hidden) * window)
+        fwd = taps[2 * order * own : (2 * order + 1) * own] * window
+        bwd = taps[(2 * order + 1) * own : (2 * order + 2) * own] * window
+        bwd = jnp.where(lag == 0, 0.0, bwd)
         plus = forward_inner(taps_layout(fwd + bwd))
         minus = forward_inner(taps_layout(fwd - bwd))
         for g in range(groups):
@@ -586,17 +611,6 @@
         )
         copy.start()
         second_sends.append(copy)
-
-    for copy in gain_sends:
-        copy.wait_recv()
-    lane = lax.broadcasted_iota(jnp.int32, (rows_n * half, LANES), 1)
-    for q in range(cols_n):
-        col_gain = column(gains[q], 0, width).reshape(rows_n, own, 1)
-        result = jnp.zeros((rows_n * half, LANES), F32)
-        for g in range(groups):
-            part = col_gain[:, g * half : (g + 1) * half].reshape(rows_n * half, 1)
-            result = jnp.where(lax.div(lane, piece) == g, part, result)
-        gain_map[q] = result
 
     for copy in copies[8:10]:
         copy.wait()
@@ -656,7 +670,7 @@
             )
             send_b[j * (LANES // piece) + h] = part.astype(BF16).reshape(rows_n, half, LANES)
     last = []
-    for step in range(1, everyone):
+    for step in sorted(range(1, everyone), key=lambda d: -min(d, everyone - d)):
         row_to, col_to = place(lax.rem(me + step, everyone))
         copy = pltpu.make_async_remote_copy(
             src_ref=send_b.at[col_to, row_to],
@@ -669,6 +683,17 @@
         copy.start()
         last.append(copy)
     recv_b[col_me, row_me] = send_b[col_me, row_me]
+
+    for copy in gain_sends:
+        copy.wait_recv()
+    lane = lax.broadcasted_iota(jnp.int32, (rows_n * half, LANES), 1)
+    for q in range(cols_n):
+        col_gain = column(gains[q], 0, width).reshape(rows_n, own, 1)
+        result = jnp.zeros((rows_n * half, LANES), F32)
+        for g in range(groups):
+            part = col_gain[:, g * half : (g + 1) * half].reshape(rows_n * half, 1)
+            result = jnp.where(lax.div(lane, piece) == g, part, result)
+        gain_map[q] = result
     for copy in copies[10:]:
         copy.wait()
     for copy in second_sends + last:
@@ -746,7 +771,7 @@
     DMA = pltpu.SemaphoreType.DMA
     return pl.pallas_call(
         functools.partial(fast_kernel, (rows_n, cols_n, block, own)),
-        out_shape=jax.ShapeDtypeStruct((piece, out_width), BF16),
+        out_shape=pltpu.VMEM((piece, out_width), BF16),
         in_specs=[hbm] * len(operands),
         out_specs=vm,
         scratch_shapes=[
@@ -769,6 +794,7 @@
             pltpu.VMEM((cols_n, 1, width), F32),
             pltpu.VMEM((cols_n, rows_n * half, LANES), F32),
             pltpu.VMEM((2, groups, rows_all, 2 * LANES), F32),
+            pltpu.VMEM((tables[-1].shape[0] // 3, embed_weight.shape[1]), F32),
             DMA((10 + groups,)),
             DMA((SMALL,)),
             DMA((2, rows_n)),

time: 26.4 us -> 24.7 us (0.936)
  local copies, waits for them, and re-layouts: 1.67 us -> 0.71 us
  Pallas kernels: 24.6 us -> 23.9 us
    unnamed x1, local copies, waits for them, and re-layouts: 1.67 us -> 0.71 us
    pallas_call x1, Pallas kernels: 24.6 us -> 23.9 us  [fast_local(): pl.pallas_call(functools.partial(fast_kernel, (rows_n, cols_n, block, own...]
where the time goes in v2:
time: 24.7 us; the launch traced here: 24.6 us
  Pallas kernels  23.9 us (97%)
  local copies, waits for them, and re-layouts  0.71 us (3%)
    pallas_call x1, Pallas kernels, fast_local(): pl.pallas_call(functools.partial(fast_kernel, (rows_n, cols_n, block, own...  23.9 us
    unnamed x1, local copies, waits for them, and re-layouts  0.71 us

profile of v2, /device:TPU:0, one launch (start us, length us, event | category | flops | bytes accessed | tf_op | source)
XLA Modules:
  0.0 24.6 jit_solution(145274316840385464)
XLA Ops:
  0.0 23.9 %shard_map.208 = bf16[64,2048]{1,0:T(8,128)(2,1)S(1)} custom-call(bf16[256,2048]{1,0:T(8,128)(2,1)} %refs_0_.1, bf16[2048,256]{1,0:T(8,128)(2,1)} %refs_1_.1, bf16[2048,256]{1,0:T(8,128)(2,1)} %refs_2_.1, bf16[2048,256]{1,0:T(8,128)(2,1)} %refs_3_.1, bf16[32,2,16,2048]{3,2,1,0:T(8,128)(2,1)} %bitcast.7, f32[1,2048]{1,0:T(1,128)} %bitcast.9, ...), custom_call_target="tpu_custom_call" | custom-call | tf_op jit(solution)/shard_map/pallas_call | solution.py:772
  23.9 0.7 %copy.24 = bf16[64,2048]{1,0:T(8,128)(2,1)} copy(bf16[64,2048]{1,0:T(8,128)(2,1)S(1)} %shard_map.208) | data formatting | bytes 524288

commit v3 on v2

--- a/solution.py
+++ b/solution.py
@@ -380,8 +380,8 @@
     loads = [
         (tokens_h, tokens_v),
         (value_h, gates_v.at[2]),
+        (first_h, gates_v.at[0]),
         (second_h, gates_v.at[1]),
-        (first_h, gates_v.at[0]),
         (feats_h, feats_v),
         (inner_h, inner_v),
         (twiddle_h, twiddle_v),
@@ -427,7 +427,7 @@
     sends = []
 
     def project(order, branch):
-        copies[1 + 2 * order].wait()
+        copies[1 + order].wait()
         gate = jnp.dot(normed_v[...], gates_v[branch], preferred_element_type=F32)
         send_a[order] = gate.T.astype(BF16).reshape(rows_n, own, block)
         if order == 0:
@@ -447,7 +447,8 @@
         recv_a[order, row_me] = send_a[order, row_me]
 
     project(0, 2)
-    copies[2].wait()
+    project(1, 0)
+    copies[3].wait()
     gate = jnp.dot(normed_v[...], gates_v[1], preferred_element_type=F32)
     gate = gate.astype(BF16).astype(F32)
     second_v[...] = gate.T
@@ -465,7 +466,6 @@
         )
         copy.start()
         halo_sends.append(copy)
-    project(1, 0)
     for copy in copies[10:]:
         copy.start()
     for copy in smalls[1:]:
@@ -578,39 +578,41 @@
             spectra[order, g, :, :LANES] = mm(p, outer_v[:, :LANES])
             spectra[order, g, :, LANES:] = mm(m, outer_v[:, LANES:])
 
-    for copy in halo_sends:
-        copy.wait_recv()
     width = rows_n * own
     count = rows_n * half
-    x = second_v[...]
-    spot = lax.broadcasted_iota(jnp.int32, (width, block), 1)
-    first_col = jnp.where(row_me == 0, 0.0, column(recv_h[1], 0, width))
-    last_col = jnp.where(row_me == rows_n - 1, 0.0, column(recv_h[0], 0, width))
-    before = jnp.where(spot == 0, first_col, pltpu.roll(x, 1, 1))
-    after = jnp.where(spot == block - 1, last_col, pltpu.roll(x, block - 1, 1))
-    w = [column(short_weight[1, j : j + 1, :], 0, width) for j in range(3)]
-    x = column(short_bias[1:2, :], 0, width) + before * w[0] + x * w[1] + after * w[2]
-    x = x.reshape(rows_n, groups, half, block)
-    for q in range(cols_n):
-        part = jnp.concatenate(
-            [x[:, g, :, q * piece : (q + 1) * piece].reshape(count, piece) for g in range(groups)],
-            axis=1,
-        )
-        send_s[q] = part.astype(BF16)
-    recv_s[col_me] = send_s[col_me]
     second_sends = []
-    for step in range(1, cols_n):
-        peer = lax.rem(col_me + step, cols_n)
-        copy = pltpu.make_async_remote_copy(
-            src_ref=send_s.at[peer],
-            dst_ref=recv_s.at[col_me],
-            send_sem=send_s_sem.at[step],
-            recv_sem=recv_s_sem.at[step],
-            device_id=(row_me, peer),
-            device_id_type=MESH,
-        )
-        copy.start()
-        second_sends.append(copy)
+
+    def send_second():
+        for copy in halo_sends:
+            copy.wait_recv()
+        x = second_v[...]
+        spot = lax.broadcasted_iota(jnp.int32, (width, block), 1)
+        first_col = jnp.where(row_me == 0, 0.0, column(recv_h[1], 0, width))
+        last_col = jnp.where(row_me == rows_n - 1, 0.0, column(recv_h[0], 0, width))
+        before = jnp.where(spot == 0, first_col, pltpu.roll(x, 1, 1))
+        after = jnp.where(spot == block - 1, last_col, pltpu.roll(x, block - 1, 1))
+        w = [column(short_weight[1, j : j + 1, :], 0, width) for j in range(3)]
+        x = column(short_bias[1:2, :], 0, width) + before * w[0] + x * w[1] + after * w[2]
+        x = x.reshape(rows_n, groups, half, block)
+        for q in range(cols_n):
+            part = jnp.concatenate(
+                [x[:, g, :, q * piece : (q + 1) * piece].reshape(count, piece) for g in range(groups)],
+                axis=1,
+            )
+            send_s[q] = part.astype(BF16)
+        recv_s[col_me] = send_s[col_me]
+        for step in range(1, cols_n):
+            peer = lax.rem(col_me + step, cols_n)
+            copy = pltpu.make_async_remote_copy(
+                src_ref=send_s.at[peer],
+                dst_ref=recv_s.at[col_me],
+                send_sem=send_s_sem.at[step],
+                recv_sem=recv_s_sem.at[step],
+                device_id=(row_me, peer),
+                device_id_type=MESH,
+            )
+            copy.start()
+            second_sends.append(copy)
 
     for copy in copies[8:10]:
         copy.wait()
@@ -654,6 +656,7 @@
         skip = to_layout(jnp.broadcast_to(skip[None], (rows_n, own, block)))
         signal = conv + signal * skip
         if order == 0:
+            send_second()
             signal = signal * smooth(1, 0)
 
     for j in range(tiles):
@@ -670,7 +673,7 @@
             )
             send_b[j * (LANES // piece) + h] = part.astype(BF16).reshape(rows_n, half, LANES)
     last = []
-    for step in sorted(range(1, everyone), key=lambda d: -min(d, everyone - d)):
+    for step in range(1, everyone):
         row_to, col_to = place(lax.rem(me + step, everyone))
         copy = pltpu.make_async_remote_copy(
             src_ref=send_b.at[col_to, row_to],

time: 24.7 us -> 23.8 us (0.964)
  Pallas kernels: 23.9 us -> 23 us
    pallas_call x1, Pallas kernels: 23.9 us -> 23 us  [fast_local(): pl.pallas_call(functools.partial(fast_kernel, (rows_n, cols_n, block, own...]
where the time goes in v3:
time: 23.8 us; the launch traced here: 23.7 us
  Pallas kernels  23 us (97%)
  local copies, waits for them, and re-layouts  0.71 us (3%)
    pallas_call x1, Pallas kernels, fast_local(): pl.pallas_call(functools.partial(fast_kernel, (rows_n, cols_n, block, own...  23 us
    unnamed x1, local copies, waits for them, and re-layouts  0.71 us

profile of v3, /device:TPU:0, one launch (start us, length us, event | category | flops | bytes accessed | tf_op | source)
XLA Modules:
  0.0 23.7 jit_solution(8070321927955282620)
XLA Ops:
  0.0 23.0 %shard_map.208 = bf16[64,2048]{1,0:T(8,128)(2,1)S(1)} custom-call(bf16[256,2048]{1,0:T(8,128)(2,1)} %refs_0_.1, bf16[2048,256]{1,0:T(8,128)(2,1)} %refs_1_.1, bf16[2048,256]{1,0:T(8,128)(2,1)} %refs_2_.1, bf16[2048,256]{1,0:T(8,128)(2,1)} %refs_3_.1, bf16[32,2,16,2048]{3,2,1,0:T(8,128)(2,1)} %bitcast.7, f32[1,2048]{1,0:T(1,128)} %bitcast.9, ...), custom_call_target="tpu_custom_call" | custom-call | tf_op jit(solution)/shard_map/pallas_call | solution.py:775
  23.0 0.7 %copy.24 = bf16[64,2048]{1,0:T(8,128)(2,1)} copy(bf16[64,2048]{1,0:T(8,128)(2,1)S(1)} %shard_map.208) | data formatting | bytes 524288

commit v4 on v3

--- a/solution.py
+++ b/solution.py
@@ -656,7 +656,6 @@
         skip = to_layout(jnp.broadcast_to(skip[None], (rows_n, own, block)))
         signal = conv + signal * skip
         if order == 0:
-            send_second()
             signal = signal * smooth(1, 0)
 
     for j in range(tiles):
@@ -686,6 +685,7 @@
         copy.start()
         last.append(copy)
     recv_b[col_me, row_me] = send_b[col_me, row_me]
+    send_second()
 
     for copy in gain_sends:
         copy.wait_recv()

time: 23.8 us -> 23.5 us (0.987)
  Pallas kernels: 23 us -> 22.6 us
    pallas_call x1, Pallas kernels: 23 us -> 22.6 us  [fast_local(): pl.pallas_call(functools.partial(fast_kernel, (rows_n, cols_n, block, own...]
where the time goes in v4:
time: 23.5 us; the launch traced here: 23.3 us
  Pallas kernels  22.6 us (96%)
  local copies, waits for them, and re-layouts  0.71 us (3%)
    pallas_call x1, Pallas kernels, fast_local(): pl.pallas_call(functools.partial(fast_kernel, (rows_n, cols_n, block, own...  22.6 us
    unnamed x1, local copies, waits for them, and re-layouts  0.71 us

profile of v4, /device:TPU:0, one launch (start us, length us, event | category | flops | bytes accessed | tf_op | source)
XLA Modules:
  0.0 23.3 jit_solution(6029320931939548931)
XLA Ops:
  0.0 22.6 %shard_map.208 = bf16[64,2048]{1,0:T(8,128)(2,1)S(1)} custom-call(bf16[256,2048]{1,0:T(8,128)(2,1)} %refs_0_.1, bf16[2048,256]{1,0:T(8,128)(2,1)} %refs_1_.1, bf16[2048,256]{1,0:T(8,128)(2,1)} %refs_2_.1, bf16[2048,256]{1,0:T(8,128)(2,1)} %refs_3_.1, bf16[32,2,16,2048]{3,2,1,0:T(8,128)(2,1)} %bitcast.7, f32[1,2048]{1,0:T(1,128)} %bitcast.9, ...), custom_call_target="tpu_custom_call" | custom-call | tf_op jit(solution)/shard_map/pallas_call | solution.py:775
  22.6 0.7 %copy.24 = bf16[64,2048]{1,0:T(8,128)(2,1)} copy(bf16[64,2048]{1,0:T(8,128)(2,1)S(1)} %shard_map.208) | data formatting | bytes 524288
